TPU v7x, 512 devices: a whole 4x4x16 slice. The times are simulated.
512 devices in a mesh: ep: 128 (over z, x, core), tp: 4 (over y).
Axes of the slice: x: 4, y: 4, z: 16, core: 2. Of those that a mesh axis runs over, the one named last changes fastest.
Arguments:
- tokens: bfloat16 [2048, 2048], P('ep', 'tp'), may hold values from -6 to 6
- state: bfloat16 [2048, 32, 4096], P('ep', 'tp'), may hold values from -6 to 6
- mix_gain: float32 [2048], P('tp'), may hold values from 0.1 to 1.9
- w_recept: bfloat16 [2048, 2048], P('tp', 'ep'), may hold values from -0.125 to 0.125
- w_key: bfloat16 [2048, 2048], P('tp', 'ep'), may hold values from -0.125 to 0.125
- w_value: bfloat16 [2048, 2048], P('tp', 'ep'), may hold values from -0.125 to 0.125
- w_decay: bfloat16 [2048, 2048], P('tp', 'ep'), may hold values from -0.125 to 0.125
- w_rate: bfloat16 [2048, 2048], P('tp', 'ep'), may hold values from -0.125 to 0.125
- decay_base: float32 [2048], P('tp'), may hold values from -4 to 2
- rate_base: float32 [2048], P('tp'), may hold values from -2 to 2
- head_gain: float32 [2048], P('tp'), may hold values from 0.1 to 1.9
- w_out: bfloat16 [2048, 2048], P('tp', 'ep'), may hold values from -0.125 to 0.125
- moe_gain: float32 [2048], replicated, may hold values from 0.1 to 1.9
- routes: int32 [2048, 6], P('ep'), may hold values from 0 to 127, all different within a row; in each aligned block of 16 rows (0 to 15, 16 to 31, ...) at most 2 rows name the same one
- route_weight: float32 [2048, 6], P('ep'), may hold values from 0.1 to 1
- expert_gate: bfloat16 [128, 2048, 512], P('ep', None, 'tp'), may hold values from -0.125 to 0.125
- expert_up: bfloat16 [128, 2048, 512], P('ep', None, 'tp'), may hold values from -0.125 to 0.125
- expert_down: bfloat16 [128, 512, 2048], P('ep', 'tp'), may hold values from -0.25 to 0.25
- shared_gate: bfloat16 [2048, 512], P(None, 'tp'), may hold values from -0.125 to 0.125
- shared_up: bfloat16 [2048, 512], P(None, 'tp'), may hold values from -0.125 to 0.125
- shared_down: bfloat16 [512, 2048], P('tp'), may hold values from -0.25 to 0.25
Outputs:
- layer_out: bfloat16 [2048, 2048], P('ep', 'tp')
Inputs may be any that keep to these rules, and one draw needn't show every extreme that they name: `routes`: each row names 6 different experts. Within the rows of one device (aligned blocks of 16 rows) no expert is named by more than 2 rows, a bound that some block reaches.
All inputs are finite; a program needn't handle non-finite values.
Results may differ from a plain program's by a relative error of at most 0.024.
Values may be sent and summed in bfloat16 or wider, within the bound.
A program may use at most 64 MiB of HBM per device.

v0:
```python
import jax
import jax.numpy as jnp
from jax import lax
from jax.sharding import Mesh
from jax.sharding import PartitionSpec as P

HEAD = 64
EP = ("ep_0", "ep_1", "ep_2")


RMS_EPS = 1e-06
GN_EPS = 0.00064
KEY_EPS = 1e-06
ROUTED_SCALE = 2.5


def cut_along(array, dim, devices):
    before, after = (array.shape[:dim], array.shape[dim + 1 :])
    return jnp.moveaxis(array.reshape(*before, devices, -1, *after), dim, 0)


def sent_and_summed(array, axis, dim):
    devices = lax.axis_size(axis)
    tiles = lax.all_to_all(cut_along(array, dim, devices), axis, 0, 0, tiled=True)
    return jnp.sum(tiles.astype(jnp.float32), axis=0)


def for_sending(array):
    return jax.tree.map(lambda a: a.astype(jnp.bfloat16) if a.dtype == jnp.float32 else a, array)


def sent_to_all(array, axis):
    copies = jnp.broadcast_to(array, (lax.axis_size(axis), *array.shape))
    return lax.all_to_all(copies, axis, split_axis=0, concat_axis=0, tiled=True)


def in_order(tiles, dim):
    lengths = list(tiles.shape[1:])
    lengths[dim] *= tiles.shape[0]
    return jnp.moveaxis(tiles, 0, dim).reshape(lengths)


def gather_axes(array, axes, dim):
    far, near = axes
    tiles = sent_to_all(sent_to_all(array, far), near)
    return in_order(tiles.swapaxes(0, 1).reshape(-1, *array.shape), dim)


def of_everyone(array, axis):
    return sent_to_all(array, axis).sum(axis=0)


def gathered_copies(array, axis, dim):
    tiles = sent_to_all(array, axis)
    return in_order(tiles, dim)


def mixer_rows(state_rows, projected, decay_base, rate_base, head_gain):
    seq_count = projected.shape[0]
    head_count = projected.shape[2] // HEAD

    def per_head(column):
        return projected[:, column, :].reshape(seq_count, head_count, HEAD)

    receptance = per_head(0)
    key_vec = per_head(1)
    value_vec = per_head(2)
    decay_pre = (projected[:, 3, :] + decay_base).reshape(seq_count, head_count, HEAD)
    rate_pre = (projected[:, 4, :] + rate_base).reshape(seq_count, head_count, HEAD)
    decay_rate = jnp.exp(-jnp.exp(-jax.nn.softplus(-decay_pre) - 0.5))
    in_rate = jax.nn.sigmoid(rate_pre)
    unit_key = key_vec * lax.rsqrt(jnp.sum(key_vec * key_vec, axis=-1, keepdims=True) + KEY_EPS)
    carried = state_rows.astype(jnp.float32).reshape(seq_count, head_count, HEAD, HEAD)
    removed = jnp.einsum("nhvk,nhk->nhv", carried, unit_key)
    updated = (
        carried * decay_rate[:, :, None, :]
        - removed[:, :, :, None] * (unit_key * in_rate)[:, :, None, :]
        + value_vec[:, :, :, None] * (key_vec * in_rate)[:, :, None, :]
    )
    readout = jnp.einsum("nhvk,nhk->nhv", updated, receptance)
    centre = jnp.mean(readout, axis=-1, keepdims=True)
    spread = jnp.mean(jnp.square(readout - centre), axis=-1, keepdims=True)
    normed = (readout - centre) * lax.rsqrt(spread + GN_EPS)
    return (normed.reshape(seq_count, head_count * HEAD) * head_gain).astype(jnp.bfloat16)


def quarter_sums(partial_value):
    return jax.tree.map(lambda part: sent_and_summed(part, "tp", 2), for_sending(partial_value))


def project_split(part_rows, weight_cols):
    inner_len = weight_cols.shape[0]
    role_count = weight_cols.shape[1]
    col_width = weight_cols.shape[2]
    flat_weight = weight_cols.reshape(inner_len, role_count * col_width)
    block_rows = gather_axes(part_rows, (("ep_0", "ep_1"), "ep_2"), 0)
    product = jnp.dot(block_rows, flat_weight, preferred_element_type=jnp.float32)
    gathered = product.astype(jnp.bfloat16).reshape(block_rows.shape[0], role_count, col_width)
    owned = lax.all_to_all(gathered, EP, split_axis=0, concat_axis=2, tiled=True)
    return quarter_sums(owned.astype(jnp.float32))


def body(
    tokens,
    state,
    mix_gain,
    w_recept,
    w_key,
    w_value,
    w_decay,
    w_rate,
    decay_base,
    rate_base,
    head_gain,
    w_out,
    moe_gain,
    routes,
    route_weight,
    expert_gate,
    expert_up,
    expert_down,
    shared_gate,
    shared_up,
    shared_down,
):
    seq_count = tokens.shape[0]
    quarter = tokens.shape[1]
    width_all = quarter * lax.axis_size("tp")
    ep_count = lax.axis_size(EP)
    topk_count = routes.shape[1]
    capacity = min(seq_count, max(2, 2 * seq_count * topk_count // ep_count))
    tokens32 = tokens.astype(jnp.float32)
    square_sum = of_everyone(jnp.sum(tokens32 * tokens32, axis=1), "tp")
    factor = lax.rsqrt(square_sum / width_all + RMS_EPS)
    normed = (tokens32 * factor[:, None] * mix_gain).astype(jnp.bfloat16)
    stacked = jnp.stack((w_recept, w_key, w_value, w_decay, w_rate), axis=1)
    projected = project_split(normed, stacked)
    mixed = mixer_rows(state, projected, decay_base, rate_base, head_gain)
    attended = project_split(mixed, w_out[:, None, :])[:, 0, :]
    resid = (tokens32 + attended).astype(jnp.bfloat16)
    full_resid = gathered_copies(resid, "tp", 1).astype(jnp.float32)
    moe_factor = lax.rsqrt(jnp.mean(full_resid * full_resid, axis=1, keepdims=True) + RMS_EPS)
    normed_two = (full_resid * moe_factor * moe_gain).astype(jnp.bfloat16)
    shared_hidden = (
        jax.nn.silu(jnp.dot(normed_two, shared_gate, preferred_element_type=jnp.float32))
        * jnp.dot(normed_two, shared_up, preferred_element_type=jnp.float32)
    ).astype(jnp.bfloat16)
    shared_part = jnp.dot(shared_hidden, shared_down, preferred_element_type=jnp.float32)
    entry_count = seq_count * topk_count
    flat_routes = routes.reshape(entry_count)
    position = jnp.arange(entry_count, dtype=jnp.int32)
    earlier = (flat_routes[:, None] == flat_routes[None, :]) & (
        position[None, :] < position[:, None]
    )
    rank_in = jnp.sum(earlier.astype(jnp.int32), axis=1)
    local_slot = flat_routes * capacity + rank_in
    slot_count = ep_count * capacity
    slot_ids = jnp.arange(slot_count, dtype=jnp.int32)
    matches = (slot_ids[:, None] == local_slot[None, :]).astype(jnp.float32)
    dispatch_map = jnp.sum(matches.reshape(slot_count, seq_count, topk_count), axis=2).astype(
        jnp.bfloat16
    )
    outgoing = jnp.dot(dispatch_map, normed_two, preferred_element_type=jnp.float32)
    outgoing = outgoing.astype(jnp.bfloat16).reshape(ep_count, capacity, width_all)
    arrived = lax.all_to_all(outgoing, EP, split_axis=0, concat_axis=0, tiled=True)
    expert_in = arrived.reshape(slot_count, width_all)
    hidden = (
        jax.nn.silu(jnp.dot(expert_in, expert_gate[0], preferred_element_type=jnp.float32))
        * jnp.dot(expert_in, expert_up[0], preferred_element_type=jnp.float32)
    ).astype(jnp.bfloat16)
    expert_part = jnp.dot(hidden, expert_down[0], preferred_element_type=jnp.float32)
    routed_sum, shared_sum = quarter_sums((expert_part[:, None, :], shared_part[:, None, :]))
    expert_out = routed_sum[:, 0, :].astype(jnp.bfloat16).reshape(ep_count, capacity, quarter)
    came_back = lax.all_to_all(expert_out, EP, split_axis=0, concat_axis=0, tiled=True).reshape(
        slot_count, quarter
    )
    picked = (
        jnp.take(came_back, local_slot, axis=0)
        .astype(jnp.float32)
        .reshape(seq_count, topk_count, quarter)
    )
    share = route_weight / jnp.sum(route_weight, axis=1, keepdims=True) * ROUTED_SCALE
    routed = jnp.sum(share[:, :, None] * picked, axis=1)
    return (resid.astype(jnp.float32) + routed + shared_sum[:, 0, :]).astype(jnp.bfloat16)


def solution(mesh):
    torus = Mesh(mesh.devices.reshape(16, 4, 2, mesh.shape["tp"]), ("ep_0", "ep_1", "ep_2", "tp"))
    placed = (
        P(EP, "tp"),
        P(EP, "tp", None),
        P("tp"),
        P("tp", EP),
        P("tp", EP),
        P("tp", EP),
        P("tp", EP),
        P("tp", EP),
        P("tp"),
        P("tp"),
        P("tp"),
        P("tp", EP),
        P(),
        P(EP, None),
        P(EP, None),
        P(EP, None, "tp"),
        P(EP, None, "tp"),
        P(EP, "tp", None),
        P(None, "tp"),
        P(None, "tp"),
        P("tp", None),
    )
    return jax.shard_map(body, mesh=torus, in_specs=placed, out_specs=P(EP, "tp"), check_vma=False)
```

profile of v0, /device:TPU:1, one launch (start us, length us, event | category | flops | bytes accessed | tf_op | source)
XLA Modules:
  0.0 399.8 jit_solution(7976692125221112094)
XLA Ops:
  0.0 0.9 fusion.33
  0.9 8.9 %all_to_all.91 = f32[4,1,16]{2,1,0:T(1,128)S(1)} all-to-all(f32[4,1,16]{2,1,0:T(1,128)S(1)} %broadcast_in_dim.19), channel_id=1, replica_groups=mesh['ep_0'=16,'ep_1'=4,'ep_2'=2,'tp'=4] {'tp'}, dimensions={0} | all-to-all | bytes 512 | tf_op jit(solution)/shard_map/all_to_all | solution.py:34
  9.9 0.8 fusion.35
  10.7 1.1 broadcast_in_dim.20
  11.8 18.3 %all-to-all-start.1 = ((bf16[64,16,512]{2,1,0:T(8,128)(2,1)}), bf16[64,16,512]{2,1,0:T(8,128)(2,1)S(1)}, u32[]{:S(2)}, u32[]{:S(2)}) async-start(bf16[64,16,512]{2,1,0:T(8,128)(2,1)} %broadcast_in_dim.20), calls=%async_computation.1 | async-start | bytes 2097152 | tf_op jit(solution)/shard_map/all_to_all | solution.py:34
  30.2 50.7 %all-to-all-done.1 = bf16[64,16,512]{2,1,0:T(8,128)(2,1)S(1)} async-done(((bf16[64,16,512]{2,1,0:T(8,128)(2,1)}), bf16[64,16,512]{2,1,0:T(8,128)(2,1)S(1)}, u32[]{:S(2)}, u32[]{:S(2)}) %all-to-all-start.1) | async-done | bytes 1048608 | tf_op jit(solution)/shard_map/all_to_all | solution.py:34
  81.3 10.4 %all_to_all.92 = bf16[2,64,16,512]{3,2,1,0:T(8,128)(2,1)S(1)} all-to-all(bf16[2,64,16,512]{3,2,1,0:T(8,128)(2,1)S(1)} %broadcast_in_dim.21), channel_id=1, replica_groups=mesh['ep_0'=16,'ep_1'=4,'ep_2'=2,'tp'=4] {'ep_2'}, dimensions={0} | all-to-all | bytes 4194304 | tf_op jit(solution)/shard_map/all_to_all | solution.py:34
  92.0 0.8 convolution_convert_fusion.2
  92.7 4.2 %copy.84 = bf16[2048,5,16]{2,1,0:T(8,128)(2,1)} copy(bf16[2048,5,16]{0,2,1:T(8,128)(2,1)S(1)} %bitcast.100) | data formatting | bytes 655360 | tf_op jit(solution)/shard_map/reshape | solution.py:98
  96.9 5.2 %reshape.273 = bf16[128,2,640]{2,1,0:T(2,128)(2,1)S(1)} reshape(bf16[2048,5,16]{2,1,0:T(8,128)(2,1)} %copy.84) | data formatting | bytes 655360
  102.1 29.0 %all_to_all.93 = bf16[128,2,640]{2,1,0:T(2,128)(2,1)S(1)} all-to-all(bf16[128,2,640]{2,1,0:T(2,128)(2,1)S(1)} %reshape.273), channel_id=1, replica_groups=mesh['ep_0'=16,'ep_1'=4,'ep_2'=2,'tp'=4] {'ep_0','ep_1','ep_2'}, dimensions={0} | all-to-all | bytes 655360 | tf_op jit(solution)/shard_map/all_to_all | solution.py:99
  131.1 4.0 reshape.274
  135.1 4.1 %copy.86 = bf16[16,5,128,16]{3,2,1,0:T(8,128)(2,1)S(1)} copy(bf16[16,5,128,16]{3,1,0,2:T(8,128)(2,1)} %bitcast.96) | data formatting | bytes 655360 | tf_op jit(solution)/shard_map/all_to_all | solution.py:99
  139.2 2.8 reshape.230
  142.1 0.8 copy.87
  142.9 3.6 all-to-all-start.4
  146.7 3.3 reshape.226
  149.9 2.5 all-to-all-done.4
  153.1 1.2 fusion.52
  154.3 2.9 fusion
  157.8 60.2 %all_to_all.94 = bf16[64,16,512]{2,1,0:T(8,128)(2,1)S(1)} all-to-all(bf16[64,16,512]{2,1,0:T(8,128)(2,1)S(1)} %broadcast_in_dim.22), channel_id=1, replica_groups=mesh['ep_0'=16,'ep_1'=4,'ep_2'=2,'tp'=4] {'ep_0','ep_1'}, dimensions={0} | all-to-all | bytes 2097152 | tf_op jit(solution)/shard_map/all_to_all | solution.py:34
  218.3 9.6 %all_to_all.95 = bf16[2,64,16,512]{3,2,1,0:T(8,128)(2,1)S(1)} all-to-all(bf16[2,64,16,512]{3,2,1,0:T(8,128)(2,1)S(1)} %broadcast_in_dim.23), channel_id=1, replica_groups=mesh['ep_0'=16,'ep_1'=4,'ep_2'=2,'tp'=4] {'ep_2'}, dimensions={0} | all-to-all | bytes 4194304 | tf_op jit(solution)/shard_map/all_to_all | solution.py:34
  228.6 0.6 fusion.7
  229.8 0.7 reduce.12
  230.8 1.0 reshape.275
  231.7 6.5 %all-to-all-start.7 = ((bf16[128,2,128]{2,1,0:T(2,128)(2,1)}), bf16[128,2,128]{2,1,0:T(2,128)(2,1)S(1)}, u32[]{:S(2)}, u32[]{:S(2)}) async-start(bf16[128,2,128]{2,1,0:T(2,128)(2,1)} %reshape.275), calls=%async_computation.7 | async-start | bytes 131072 | tf_op jit(solution)/shard_map/all_to_all | solution.py:99
  238.7 14.4 %all-to-all-done.7 = bf16[128,2,128]{2,1,0:T(2,128)(2,1)S(1)} async-done(((bf16[128,2,128]{2,1,0:T(2,128)(2,1)}), bf16[128,2,128]{2,1,0:T(2,128)(2,1)S(1)}, u32[]{:S(2)}, u32[]{:S(2)}) %all-to-all-start.7) | async-done | bytes 65568 | tf_op jit(solution)/shard_map/all_to_all | solution.py:99
  253.1 0.9 reshape.276
  254.9 1.1 copy.92
  256.6 0.6 copy.93
  257.2 3.3 all-to-all-start.8
  260.6 4.3 %all-to-all-done.8 = bf16[4,16,1,512]{3,1,2,0:T(8,128)(2,1)S(1)} async-done(((bf16[4,16,1,512]{3,1,2,0:T(8,128)(2,1)}), bf16[4,16,1,512]{3,1,2,0:T(8,128)(2,1)S(1)}, u32[]{:S(2)}, u32[]{:S(2)}) %all-to-all-start.8) | async-done | bytes 65568 | tf_op jit(solution)/shard_map/all_to_all | solution.py:24
  265.6 3.3 all-to-all-start.9
  269.0 4.4 %all-to-all-done.9 = bf16[4,16,512]{2,1,0:T(8,128)(2,1)S(1)} async-done(((bf16[4,16,512]{2,1,0:T(8,128)(2,1)}), bf16[4,16,512]{2,1,0:T(8,128)(2,1)S(1)}, u32[]{:S(2)}, u32[]{:S(2)}) %all-to-all-start.9) | async-done | bytes 65568 | tf_op jit(solution)/shard_map/all_to_all | solution.py:34
  274.1 0.7 reshape.235
  274.8 60.4 %all_to_all.96 = bf16[128,2,2048]{2,1,0:T(2,128)(2,1)} all-to-all(bf16[128,2,2048]{2,1,0:T(2,128)(2,1)S(1)} %reshape.235), channel_id=1, replica_groups=mesh['ep_0'=16,'ep_1'=4,'ep_2'=2,'tp'=4] {'ep_0','ep_1','ep_2'}, dimensions={0} | all-to-all | bytes 2097152 | tf_op jit(solution)/shard_map/all_to_all | solution.py:165
  335.2 1.6 reshape.236
  337.3 0.8 convolution_convert_fusion
  338.0 0.8 reshape.237
  338.9 1.2 copy.121
  340.1 3.5 all-to-all-start.11
  344.8 11.8 %all-to-all-done.11 = bf16[4,256,1,512]{3,1,2,0:T(8,128)(2,1)S(1)} async-done(((bf16[4,256,1,512]{3,1,2,0:T(8,128)(2,1)}), bf16[4,256,1,512]{3,1,2,0:T(8,128)(2,1)S(1)}, u32[]{:S(2)}, u32[]{:S(2)}) %all-to-all-start.11) | async-done | bytes 1048608 | tf_op jit(solution)/shard_map/all_to_all | solution.py:24
  356.7 3.3 all-to-all-start.13
  360.2 0.8 convert_element_type.111
  361.0 3.4 all-to-all-done.13
  364.4 13.3 %all-to-all-start.12 = ((bf16[128,2,512]{2,1,0:T(2,128)(2,1)}), bf16[128,2,512]{2,1,0:T(2,128)(2,1)S(1)}, u32[]{:S(2)}, u32[]{:S(2)}) async-start(bf16[128,2,512]{2,1,0:T(2,128)(2,1)} %convert_element_type.111), calls=%async_computation.12 | async-start | bytes 524288 | tf_op jit(solution)/shard_map/all_to_all | solution.py:174
  377.9 20.2 %all-to-all-done.12 = bf16[128,2,512]{2,1,0:T(2,128)(2,1)S(1)} async-done(((bf16[128,2,512]{2,1,0:T(2,128)(2,1)}), bf16[128,2,512]{2,1,0:T(2,128)(2,1)S(1)}, u32[]{:S(2)}, u32[]{:S(2)}) %all-to-all-start.12) | async-done | bytes 262176 | tf_op jit(solution)/shard_map/all_to_all | solution.py:174
  398.2 0.8 gather_fusion
  (109 shorter events, 10.2 us)
Async XLA Ops:
  0.0 337.2 %copy-start = (bf16[1,128,2048]{2,1,0:T(8,128)(2,1)S(1)}, bf16[1,128,2048]{2,1,0:T(8,128)(2,1)}, u32[]{:S(2)}) copy-start(bf16[1,128,2048]{2,1,0:T(8,128)(2,1)} %param.38) | copy-start | bytes 1572868
  0.0 30.1 %copy-start.9 = (bf16[512,16]{0,1:T(8,128)(2,1)S(1)}, bf16[512,16]{0,1:T(8,128)(2,1)}, u32[]{:S(2)}) copy-start(bf16[512,16]{0,1:T(8,128)(2,1)} %param.24) | copy-start | bytes 49156
  0.0 30.1 %copy-start.10 = (bf16[512,16]{0,1:T(8,128)(2,1)S(1)}, bf16[512,16]{0,1:T(8,128)(2,1)}, u32[]{:S(2)}) copy-start(bf16[512,16]{0,1:T(8,128)(2,1)} %param.25) | copy-start | bytes 49156
  0.0 30.1 %copy-start.11 = (bf16[512,16]{0,1:T(8,128)(2,1)S(1)}, bf16[512,16]{0,1:T(8,128)(2,1)}, u32[]{:S(2)}) copy-start(bf16[512,16]{0,1:T(8,128)(2,1)} %param.26) | copy-start | bytes 49156
  0.0 30.2 %copy-start.12 = (bf16[512,16]{0,1:T(8,128)(2,1)S(1)}, bf16[512,16]{0,1:T(8,128)(2,1)}, u32[]{:S(2)}) copy-start(bf16[512,16]{0,1:T(8,128)(2,1)} %param.27) | copy-start | bytes 49156
  0.0 30.2 %copy-start.13 = (bf16[512,16]{0,1:T(8,128)(2,1)S(1)}, bf16[512,16]{0,1:T(8,128)(2,1)}, u32[]{:S(2)}) copy-start(bf16[512,16]{0,1:T(8,128)(2,1)} %param.28) | copy-start | bytes 49156
  11.8 69.1 %all-to-all-start.1 = ((bf16[64,16,512]{2,1,0:T(8,128)(2,1)}), bf16[64,16,512]{2,1,0:T(8,128)(2,1)S(1)}, u32[]{:S(2)}, u32[]{:S(2)}) async-start(bf16[64,16,512]{2,1,0:T(8,128)(2,1)} %broadcast_in_dim.20), calls=%async_computation.1 | async-start | bytes 2097152 | tf_op jit(solution)/shard_map/all_to_all | solution.py:34
  139.2 7.3 %copy-start.16 = (f32[512]{0:T(512)S(1)}, f32[512]{0:T(512)}, u32[]{:S(2)}) copy-start(f32[512]{0:T(512)} %param.29) | copy-start | bytes 6148
  139.2 7.4 %copy-start.17 = (f32[512]{0:T(512)S(1)}, f32[512]{0:T(512)}, u32[]{:S(2)}) copy-start(f32[512]{0:T(512)} %param.30) | copy-start | bytes 6148
  142.9 9.6 %all-to-all-start.4 = ((bf16[4,16,5,512]{3,1,2,0:T(8,128)(2,1)}), bf16[4,16,5,512]{3,1,2,0:T(8,128)(2,1)S(1)}, u32[]{:S(2)}, u32[]{:S(2)}) async-start(bf16[4,16,5,512]{3,1,2,0:T(8,128)(2,1)} %copy.87), calls=%async_computation.4 | async-start | bytes 655360 | tf_op jit(solution)/shard_map/all_to_all | solution.py:24
  154.3 3.4 copy-start.18
  227.9 0.7 copy-start.7
  228.2 10.1 %copy-start.15 = (s32[16,6]{0,1:T(8,128)S(1)}, s32[16,6]{0,1:T(8,128)}, u32[]{:S(2)}) copy-start(s32[16,6]{0,1:T(8,128)} %param.34) | copy-start | bytes 1156
  231.7 21.4 %all-to-all-start.7 = ((bf16[128,2,128]{2,1,0:T(2,128)(2,1)}), bf16[128,2,128]{2,1,0:T(2,128)(2,1)S(1)}, u32[]{:S(2)}, u32[]{:S(2)}) async-start(bf16[128,2,128]{2,1,0:T(2,128)(2,1)} %reshape.275), calls=%async_computation.7 | async-start | bytes 131072 | tf_op jit(solution)/shard_map/all_to_all | solution.py:99
  254.0 11.0 %copy-start.6 = (bf16[16,512]{1,0:T(8,128)(2,1)S(1)}, bf16[16,512]{1,0:T(8,128)(2,1)}, u32[]{:S(2)}) copy-start(bf16[16,512]{1,0:T(8,128)(2,1)} %param.21) | copy-start | bytes 49156
  254.0 19.5 %copy-start.14 = (f32[2048]{0:T(1024)S(1)}, f32[2048]{0:T(1024)}, u32[]{:S(2)}) copy-start(f32[2048]{0:T(1024)} %param.33) | copy-start | bytes 24580
  257.2 7.7 %all-to-all-start.8 = ((bf16[4,16,1,512]{3,1,2,0:T(8,128)(2,1)}), bf16[4,16,1,512]{3,1,2,0:T(8,128)(2,1)S(1)}, u32[]{:S(2)}, u32[]{:S(2)}) async-start(bf16[4,16,1,512]{3,1,2,0:T(8,128)(2,1)} %copy.93), calls=%async_computation.8 | async-start | bytes 131072 | tf_op jit(solution)/shard_map/all_to_all | solution.py:24
  265.6 7.7 %all-to-all-start.9 = ((bf16[4,16,512]{2,1,0:T(8,128)(2,1)}), bf16[4,16,512]{2,1,0:T(8,128)(2,1)S(1)}, u32[]{:S(2)}, u32[]{:S(2)}) async-start(bf16[4,16,512]{2,1,0:T(8,128)(2,1)} %broadcast_in_dim.25), calls=%async_computation.9 | async-start | bytes 131072 | tf_op jit(solution)/shard_map/all_to_all | solution.py:34
  335.2 1.6 copy-start.5
  335.2 2.0 copy-start.1
  338.8 4.7 %copy-start.4 = (bf16[2048,128]{1,0:T(8,128)(2,1)S(1)}, bf16[2048,128]{1,0:T(8,128)(2,1)}, u32[]{:S(2)}) copy-start(bf16[2048,128]{1,0:T(8,128)(2,1)} %param.39) | copy-start | bytes 1572868
  338.9 4.9 %copy-start.2 = (bf16[128,2048]{1,0:T(8,128)(2,1)S(1)}, bf16[128,2048]{1,0:T(8,128)(2,1)}, u32[]{:S(2)}) copy-start(bf16[128,2048]{1,0:T(8,128)(2,1)} %param.41) | copy-start | bytes 1572868
  338.9 4.9 %copy-start.3 = (bf16[2048,128]{1,0:T(8,128)(2,1)S(1)}, bf16[2048,128]{1,0:T(8,128)(2,1)}, u32[]{:S(2)}) copy-start(bf16[2048,128]{1,0:T(8,128)(2,1)} %param.40) | copy-start | bytes 1572868
  340.1 16.6 %all-to-all-start.11 = ((bf16[4,256,1,512]{3,1,2,0:T(8,128)(2,1)}), bf16[4,256,1,512]{3,1,2,0:T(8,128)(2,1)S(1)}, u32[]{:S(2)}, u32[]{:S(2)}) async-start(bf16[4,256,1,512]{3,1,2,0:T(8,128)(2,1)} %bitcast.94), calls=%async_computation.11 | async-start | bytes 2097152 | tf_op jit(solution)/shard_map/all_to_all | solution.py:24
  343.8 34.0 %copy-start.8 = (f32[16,6]{0,1:T(8,128)S(1)}, f32[16,6]{0,1:T(8,128)}, u32[]{:S(2)}) copy-start(f32[16,6]{0,1:T(8,128)} %param.35) | copy-start | bytes 1156
  356.7 7.7 %all-to-all-start.13 = ((bf16[4,16,1,512]{3,1,2,0:T(8,128)(2,1)}), bf16[4,16,1,512]{3,1,2,0:T(8,128)(2,1)S(1)}, u32[]{:S(2)}, u32[]{:S(2)}) async-start(bf16[4,16,1,512]{3,1,2,0:T(8,128)(2,1)} %bitcast.95), calls=%async_computation.13 | async-start | bytes 131072 | tf_op jit(solution)/shard_map/all_to_all | solution.py:24
  364.4 33.7 %all-to-all-start.12 = ((bf16[128,2,512]{2,1,0:T(2,128)(2,1)}), bf16[128,2,512]{2,1,0:T(2,128)(2,1)S(1)}, u32[]{:S(2)}, u32[]{:S(2)}) async-start(bf16[128,2,512]{2,1,0:T(2,128)(2,1)} %convert_element_type.111), calls=%async_computation.12 | async-start | bytes 524288 | tf_op jit(solution)/shard_map/all_to_all | solution.py:174
where the time goes:
time: 402 us; the launch traced here: 400 us
  blocking collectives  179 us (45%)
  waiting for transfers between devices  112 us (28%)
  starting transfers between devices  55.1 us (14%)
  local copies, waits for them, and re-layouts  41.4 us (10%)
  matrix products  7.65 us (2%)
  other arithmetic  4.57 us (1%)
    all_to_all x4, blocking collectives, sent_to_all(): return lax.all_to_all(copies, axis, split_axis=0, concat_axis=0, tiled=True)  89.2 us
    all_to_all x1, blocking collectives, body(): lax.all_to_all(outgoing, EP, split_axis=0, concat_axis=0, tiled=True)  60.4 us
    all_to_all x2, waiting for transfers between devices, sent_to_all(): return lax.all_to_all(copies, axis, split_axis=0, concat_axis=0, tiled=True)  55.1 us
    all_to_all x1, blocking collectives, project_split(): lax.all_to_all(gathered, EP, split_axis=0, concat_axis=2, tiled=True)  29 us
    all_to_all x4, waiting for transfers between devices, sent_and_summed(): lax.all_to_all(cut_along(array, dim, devices), axis, 0, 0, tiled=True)  22.1 us
    all_to_all x2, starting transfers between devices, sent_to_all(): return lax.all_to_all(copies, axis, split_axis=0, concat_axis=0, tiled=True)  21.6 us
    all_to_all x1, waiting for transfers between devices, body(): lax.all_to_all(expert_out, EP, split_axis=0, concat_axis=0, tiled=True)  20.2 us
    all_to_all x1, waiting for transfers between devices, project_split(): lax.all_to_all(gathered, EP, split_axis=0, concat_axis=2, tiled=True)  14.4 us
  transfers between devices with their start and end apart: 8, of which 8 were waited for; matrix products, arithmetic and copies ran while one was open for 2% of the time, Pallas kernels for 0%

commit v1 on v0

v1 whole, which is shorter than its diff:
```python
import functools

import jax
import jax.numpy as jnp
from jax import lax
from jax.experimental import pallas as pl
from jax.experimental.pallas import tpu as pltpu
from jax.sharding import Mesh
from jax.sharding import PartitionSpec as P

HEAD = 64
LANES = 128
RMS_EPS = 1e-06
GN_EPS = 0.00064
KEY_EPS = 1e-06
ROUTED_SCALE = 2.5
AXES = ("ep_0", "ep_1", "ep_2", "tp")
EP = AXES[:3]
MESH_ID = pl.DeviceIdType.MESH
F32 = jnp.float32
BF16 = jnp.bfloat16
NT = (((1,), (1,)), ((), ()))
TN = (((0,), (0,)), ((), ()))


def iota(shape, dim):
    return lax.broadcasted_iota(jnp.int32, shape, dim)


def mm(a, b):
    return jnp.dot(a, b, preferred_element_type=F32)


def silu(v):
    return v * jax.nn.sigmoid(v)


def layer(
    sizes,
    tok, w0, w1, w2, w3, w4, w5, state, mix_gain, decay_base, rate_base, head_gain, moe_gain, routing,
    gate_hbm, up_hbm, down_hbm, sgate_hbm, sup_hbm, sdown_hbm,
    out,
    wbuf, xs, xg, tg, gt, ut, dt, vs, vg, perm, seg, st, nh, prod,
    ps, pr, ms, mg, ao, ar, resid, ns, zg, sgv, suv, sdv, sh, shr,
    dmat, cmat, xsel, er, gs, gr, hs, hr, ob, cb, rb, zr,
    s_send, s_ring, s_xg, s_tg, s_gt, s_ut, s_dt, s_vg, s_pr, s_mg, s_ar, s_zg, s_shr, s_er, s_gr, s_hr, s_cb, s_zr,
    s_loc,
):
    nz, nx, nc, ny = sizes
    nxc = nx * nc
    rows, q = tok.shape
    zb = nz // ny
    heads = q // HEAD
    topk = routing.shape[0] // 2
    weights = (w0, w1, w2, w3, w4, w5)
    z, x, c, y = (lax.axis_index(a) for a in AXES)
    xc = x * nc + c
    sends = []

    def send(src, dst, recv_sem, where):
        copy = pltpu.make_async_remote_copy(
            src_ref=src, dst_ref=dst, send_sem=s_send.at[len(sends)], recv_sem=recv_sem,
            device_id=where, device_id_type=MESH_ID,
        )
        copy.start()
        sends.append(copy)

    def arrived(dst, recv_sem):
        pltpu.make_async_remote_copy(
            src_ref=dst, dst_ref=dst, send_sem=s_send.at[0], recv_sem=recv_sem,
            device_id=(z, x, c, y), device_id_type=MESH_ID,
        ).wait_recv()

    xc_off = [(dx, dc) for dx in range(nx) for dc in range(nc)]

    def xc_at(off):
        px, pc = lax.rem(x + off[0], nx), lax.rem(c + off[1], nc)
        return px, pc, px * nc + pc

    def y_at(dy):
        return lax.rem(y + dy, ny)

    def z_at(dz):
        return lax.rem(z + dz, nz)

    plane_off = [(o, dy) for o in xc_off for dy in range(ny)][1:]

    def at_lanes(i):
        return pl.ds(pl.multiple_of(i * LANES, LANES), LANES)

    local = []

    def load(src, dst):
        copy = pltpu.make_async_copy(src, dst, s_loc.at[len(local)])
        copy.start()
        local.append(copy)
        return copy

    own_rows = pl.ds(pl.multiple_of(y * q, q), q)
    load_gate = load(gate_hbm.at[own_rows, :], gt.at[y])
    load_up = load(up_hbm.at[own_rows, :], ut.at[y])
    load_down = load(down_hbm.at[:, own_rows], dt.at[y])
    load_state = load(state, st)
    load_sg = load(sgate_hbm, sgv)
    load_su = load(sup_hbm, suv)
    load_sd = load(sdown_hbm, sdv)

    tok32 = tok[...].astype(F32)
    rows_in = (tok32 * mix_gain[...]).astype(BF16)
    xs[...] = rows_in
    xg[xc] = rows_in
    tg[y] = tok[...]
    for m in range(6):
        wbuf[z // zb, m, lax.rem(z, zb)] = weights[m][...]

    barrier = pltpu.get_barrier_semaphore()
    for off, dy in plane_off:
        px, pc, _ = xc_at(off)
        pl.semaphore_signal(barrier, inc=1, device_id=(z, px, pc, y_at(dy)), device_id_type=MESH_ID)
    for dz in range(1, nz):
        pl.semaphore_signal(barrier, inc=1, device_id=(z_at(dz), x, c, y), device_id_type=MESH_ID)
    pl.semaphore_wait(barrier, len(plane_off) + nz - 1)

    half = nz // 2
    to_next, to_prev = (z_at(1), x, c, y), (z_at(nz - 1), x, c, y)
    for m in range(6):
        spot = wbuf.at[z // zb, m, lax.rem(z, zb)]
        send(weights[m], spot, s_ring.at[0, 0, m], to_next)
        send(weights[m], spot, s_ring.at[1, 0, m], to_prev)
    for off in xc_off[1:]:
        px, pc, _ = xc_at(off)
        send(xs, xg.at[xc], s_xg.at[xc], (z, px, pc, y))
    for dy in range(1, ny):
        send(tok, tg.at[y], s_tg.at[y], (z, x, c, y_at(dy)))
    for dy in range(1, ny):
        theirs = pl.ds(pl.multiple_of(y_at(dy) * q, q), q)
        send(gate_hbm.at[theirs, :], gt.at[y], s_gt.at[y], (z, x, c, y_at(dy)))
        send(up_hbm.at[theirs, :], ut.at[y], s_ut.at[y], (z, x, c, y_at(dy)))

    score = routing[topk : 2 * topk, :]
    share = score / jnp.sum(score, axis=0, keepdims=True) * ROUTED_SCALE
    experts = vs.shape[0]
    lane = iota((experts, LANES), 1)
    expert_id = iota((experts, LANES), 0).astype(F32)
    value = jnp.zeros((experts, LANES), F32)
    for k in range(topk):
        value += jnp.where(expert_id == routing[k : k + 1, :], share[k : k + 1, :], 0.0)
    same_block = (iota((LANES, LANES), 0) // rows == iota((LANES, LANES), 1) // rows) & (
        iota((LANES, LANES), 0) < iota((LANES, LANES), 1)
    )
    before = mm((value > 0.0).astype(BF16), same_block.astype(BF16))
    signed = jnp.where(before > 0.5, -value, value)
    vs[...] = jnp.where(lane // rows == lax.rem(z, LANES // rows), signed, 0.0)

    width = nxc * LANES
    strip = nxc * 16
    for i in range(nxc):
        r = iota((LANES, width), 0)
        goal = (r // 16) * strip + i * 16 + lax.rem(r, 16)
        perm[i * LANES : (i + 1) * LANES, :] = (iota((LANES, width), 1) == goal).astype(BF16)
    for j in range(HEAD // 2):
        r = iota((LANES, LANES), 0)
        goal = 2 * j + r // HEAD
        seg[j * LANES : (j + 1) * LANES, :] = (lax.rem(iota((LANES, LANES), 1), HEAD) == goal).astype(BF16)

    for step in range(1, half + 1):
        up_src, down_src = z_at(nz - step), z_at(step)
        for m in range(6):
            if step < half or m < 3:
                spot = wbuf.at[up_src // zb, m, lax.rem(up_src, zb)]
                arrived(spot, s_ring.at[0, step - 1, m])
                if step + 1 < half or (step + 1 == half and m < 3):
                    send(spot, spot, s_ring.at[0, step, m], to_next)
            if step < half or m >= 3:
                spot = wbuf.at[down_src // zb, m, lax.rem(down_src, zb)]
                arrived(spot, s_ring.at[1, step - 1, m])
                if step + 1 < half or (step + 1 == half and m >= 3):
                    send(spot, spot, s_ring.at[1, step, m], to_prev)
        if step == 1:
            for dz in range(1, nz):
                zt = z_at(dz)
                send(vs.at[pl.ds(pl.multiple_of(zt * nxc, nxc), nxc), :], vg.at[z], s_vg.at[z], (zt, x, c, y))
            vg[z] = vs[pl.ds(pl.multiple_of(z * nxc, nxc), nxc), :]

    for off in xc_off[1:]:
        _, _, pxc = xc_at(off)
        arrived(xg.at[pxc], s_xg.at[pxc])
    left = xg[...].reshape(nxc * rows, q)
    for yt in range(ny):
        for pair in range(3):
            w = wbuf[yt, 2 * pair : 2 * pair + 2].reshape(LANES, q)
            part = lax.dot_general(left, w, NT, preferred_element_type=F32)
            ps[yt, :, pair] = part.astype(BF16).reshape(nxc, rows, LANES)
    for off, dy in plane_off:
        px, pc, pxc = xc_at(off)
        py = y_at(dy)
        send(ps.at[py, pxc], pr.at[y, :, :, at_lanes(xc)], s_pr.at[xc * ny + y], (z, px, pc, py))
    for dy in range(1, ny):
        theirs = pl.ds(pl.multiple_of(y_at(dy) * q, q), q)
        send(down_hbm.at[:, theirs], dt.at[y], s_dt.at[y], (z, x, c, y_at(dy)))
    pr[y, :, :, at_lanes(xc)] = ps[y, xc]

    for dy in range(1, ny):
        arrived(tg.at[y_at(dy)], s_tg.at[y_at(dy)])
    tok_all = tg[...].astype(F32)
    square = jnp.sum(jnp.sum(tok_all * tok_all, axis=0), axis=1, keepdims=True)
    factor = lax.rsqrt(square / (ny * q) + RMS_EPS)

    for off, dy in plane_off:
        _, _, pxc = xc_at(off)
        arrived(pr.at[y_at(dy), :, :, at_lanes(pxc)], s_pr.at[pxc * ny + y_at(dy)])
    spread = mm(pr[...].reshape(ny * 3 * rows, width), perm[...]).reshape(ny, 3, rows, width)
    summed = jnp.sum(spread, axis=0)
    low = iota((rows, LANES), 1) < HEAD
    for m in range(5):
        flat = summed[m // 2, :, (m % 2) * q : (m % 2 + 1) * q] * factor
        if m == 3:
            flat = flat + decay_base[...]
        if m == 4:
            flat = flat + rate_base[...]
        for t in range(q // LANES):
            here = flat[:, t * LANES : (t + 1) * LANES]
            swapped = pltpu.roll(here, HEAD, 1)
            nh[m, pl.ds(2 * t, rows, stride=heads), :] = jnp.where(low, here, swapped)
            nh[m, pl.ds(2 * t + 1, rows, stride=heads), :] = jnp.where(low, swapped, here)

    def head_sum(v):
        return 0.5 * jnp.sum(v, axis=1, keepdims=True)

    receptance, key, val = nh[0], nh[1], nh[2]
    decay = jnp.exp(-jnp.exp(-jax.nn.softplus(-nh[3]) - 0.5))
    in_rate = jax.nn.sigmoid(nh[4])
    unit = key * lax.rsqrt(head_sum(key * key) + KEY_EPS)
    rated = in_rate * receptance
    mix_w = decay * receptance - head_sum(unit * rated) * unit
    fed = head_sum(key * rated)
    load_state.wait()
    for j in range(HEAD // 2):
        block = st[:, :, j * LANES : (j + 1) * LANES].astype(F32).reshape(rows * heads, LANES)
        prod[:, j * LANES : (j + 1) * LANES] = (block * mix_w).astype(BF16)
    readout = mm(prod[...], seg[...]) + fed * val
    centre = jnp.sum(readout, axis=1, keepdims=True) / LANES
    moved = readout - centre
    var = jnp.sum(moved * moved, axis=1, keepdims=True) / LANES
    nh[0] = moved * lax.rsqrt(var + GN_EPS)
    for t in range(q // LANES):
        even = nh[0, pl.ds(2 * t, rows, stride=heads), :]
        odd = nh[0, pl.ds(2 * t + 1, rows, stride=heads), :]
        cols = slice(t * LANES, (t + 1) * LANES)
        ms[:, cols] = (jnp.where(low, even, odd) * head_gain[:, cols]).astype(BF16)

    for off in xc_off[1:]:
        px, pc, _ = xc_at(off)
        send(ms, mg.at[xc], s_mg.at[xc], (z, px, pc, y))
    mg[xc] = ms[...]
    for off in xc_off[1:]:
        _, _, pxc = xc_at(off)
        arrived(mg.at[pxc], s_mg.at[pxc])
    left = mg[...].reshape(nxc * rows, q)
    per = 8 // zb
    for zh in range(nz // 8):
        w = wbuf[per * zh : per * (zh + 1), 5].reshape(LANES, q)
        part = lax.dot_general(left, w, NT, preferred_element_type=F32)
        ao[:, zh] = part.astype(BF16).reshape(nxc, rows, LANES)
    for off, dy in plane_off:
        px, pc, pxc = xc_at(off)
        send(ao.at[pxc], ar.at[y, :, :, at_lanes(xc)], s_ar.at[xc * ny + y], (z, px, pc, y_at(dy)))
    ar[y, :, :, at_lanes(xc)] = ao[xc]
    for off, dy in plane_off:
        _, _, pxc = xc_at(off)
        arrived(ar.at[y_at(dy), :, :, at_lanes(pxc)], s_ar.at[pxc * ny + y_at(dy)])
    spread = mm(ar[...].reshape(ny * (nz // 8) * rows, width), perm[...]).reshape(ny, nz // 8, rows, width)
    summed = jnp.sum(spread, axis=0)
    per = width // q
    square = jnp.zeros((rows, 1), F32)
    for i in range(ny):
        attended = summed[i // per, :, (i % per) * q : (i % per + 1) * q]
        resid[i] = (tg[i].astype(F32) + attended).astype(BF16)
        r32 = resid[i].astype(F32)
        square += jnp.sum(r32 * r32, axis=1, keepdims=True)
    factor = lax.rsqrt(square / (ny * q) + RMS_EPS)
    for i in range(ny):
        ns[i] = (resid[i].astype(F32) * factor * moe_gain[:, i * q : (i + 1) * q]).astype(BF16)

    for dz in range(1, nz):
        send(ns.at[y], zg.at[z], s_zg.at[z], (z_at(dz), x, c, y))
    zg[z] = ns[y]

    load_sg.wait()
    load_su.wait()
    load_sd.wait()
    hid_g = jnp.zeros((rows, LANES), F32)
    hid_u = jnp.zeros((rows, LANES), F32)
    for i in range(ny):
        hid_g += mm(ns[i], sgv[i * q : (i + 1) * q, :])
        hid_u += mm(ns[i], suv[i * q : (i + 1) * q, :])
    hid = (silu(hid_g) * hid_u).astype(BF16)
    for i in range(ny):
        sh[i] = mm(hid, sdv[:, i * q : (i + 1) * q]).astype(BF16)
    for dy in range(1, ny):
        send(sh.at[y_at(dy)], shr.at[y], s_shr.at[y], (z, x, c, y_at(dy)))
    shr[y] = sh[y]

    for dz in range(1, nz):
        arrived(vg.at[z_at(dz)], s_vg.at[z_at(dz)])
    per = LANES // rows
    table = jnp.concatenate([jnp.sum(vg[h * per : (h + 1) * per], axis=0) for h in range(nz // per)], axis=1)
    shape = (2 * nz, nz * rows)
    mine = iota(shape, 0) // 2 == iota(shape, 1) // rows
    sign = jnp.where(lax.rem(iota(shape, 0), 2) == 0, 1.0, -1.0)
    for i in range(nxc):
        weight = jnp.where(mine, table[i : i + 1, :] * sign, 0.0)
        spot = slice(i * 2 * nz, (i + 1) * 2 * nz)
        dmat[spot, :] = (weight > 0.0).astype(BF16)
        cmat[spot, :] = jnp.maximum(weight, 0.0).astype(BF16)

    for dz in range(1, nz):
        arrived(zg.at[z_at(dz)], s_zg.at[z_at(dz)])
    picked = mm(dmat[...], zg[...].reshape(nz * rows, q)).astype(BF16)
    xsel[...] = picked.reshape(nxc, 2 * nz, q)
    for off in xc_off[1:]:
        px, pc, pxc = xc_at(off)
        send(xsel.at[pxc], er.at[xc], s_er.at[xc], (z, px, pc, y))
    er[xc] = xsel[xc]

    load_gate.wait()
    load_up.wait()
    load_down.wait()
    for dy in range(1, ny):
        arrived(gt.at[y_at(dy)], s_gt.at[y_at(dy)])
        arrived(ut.at[y_at(dy)], s_ut.at[y_at(dy)])
        arrived(dt.at[y_at(dy)], s_dt.at[y_at(dy)])
    for off in xc_off[1:]:
        _, _, pxc = xc_at(off)
        arrived(er.at[pxc], s_er.at[pxc])
    chosen = er[...].reshape(nxc * 2 * nz, q)
    for i in range(ny):
        gs[i, :, 0:LANES] = mm(chosen, gt[i]).astype(BF16)
        gs[i, :, LANES : 2 * LANES] = mm(chosen, ut[i]).astype(BF16)
    for dy in range(1, ny):
        send(gs.at[y_at(dy)], gr.at[y], s_gr.at[y], (z, x, c, y_at(dy)))
    gr[y] = gs[y]
    for dy in range(1, ny):
        arrived(gr.at[y_at(dy)], s_gr.at[y_at(dy)])
    pre = jnp.sum(gr[...].astype(F32), axis=0)
    hs[...] = (silu(pre[:, 0:LANES]) * pre[:, LANES : 2 * LANES]).astype(BF16)
    for dy in range(1, ny):
        send(hs, hr.at[y], s_hr.at[y], (z, x, c, y_at(dy)))
    hr[y] = hs[...]
    for dy in range(1, ny):
        arrived(hr.at[y_at(dy)], s_hr.at[y_at(dy)])
    total = mm(hr[0], dt[0])
    for i in range(1, ny):
        total += mm(hr[i], dt[i])
    ob[...] = total.astype(BF16).reshape(nxc, 2 * nz, q)
    for off in xc_off[1:]:
        px, pc, pxc = xc_at(off)
        send(ob.at[pxc], cb.at[xc], s_cb.at[xc], (z, px, pc, y))
    cb[xc] = ob[xc]
    for off in xc_off[1:]:
        _, _, pxc = xc_at(off)
        arrived(cb.at[pxc], s_cb.at[pxc])

    routed = lax.dot_general(cmat[...], cb[...].reshape(nxc * 2 * nz, q), TN, preferred_element_type=F32)
    rb[...] = routed.astype(BF16).reshape(nz, rows, q)
    for dz in range(1, nz):
        send(rb.at[z_at(dz)], zr.at[z], s_zr.at[z], (z_at(dz), x, c, y))
    zr[z] = rb[z]
    for dy in range(1, ny):
        arrived(shr.at[y_at(dy)], s_shr.at[y_at(dy)])
    for dz in range(1, nz):
        arrived(zr.at[z_at(dz)], s_zr.at[z_at(dz)])
    final = resid[y].astype(F32) + jnp.sum(zr[...].astype(F32), axis=0) + jnp.sum(shr[...].astype(F32), axis=0)
    out[...] = final.astype(BF16)
    for copy in sends:
        copy.wait_send()


def body(
    tokens, state, mix_gain, w_recept, w_key, w_value, w_decay, w_rate, decay_base, rate_base, head_gain, w_out,
    moe_gain, routes, route_weight, expert_gate, expert_up, expert_down, shared_gate, shared_up, shared_down,
):
    sizes = tuple(lax.axis_size(a) for a in AXES)
    nz, nx, nc, ny = sizes
    nxc = nx * nc
    rows, q = tokens.shape
    heads = q // HEAD
    routing = jnp.concatenate([routes.T.astype(F32), route_weight.T], axis=0)
    routing = jnp.tile(routing, (1, LANES // rows))
    turned = [w.T for w in (w_recept, w_key, w_value, w_decay, w_rate, w_out)]
    line = [v[None, :] for v in (mix_gain, decay_base, rate_base, head_gain, moe_gain)]
    vmem = pl.BlockSpec(memory_space=pltpu.VMEM)
    hbm = pl.BlockSpec(memory_space=pl.ANY)
    slots = 2 * nz
    count = nxc * slots
    width = nxc * LANES

    def vb(*shape):
        return pltpu.VMEM(shape, BF16)

    def vf(*shape):
        return pltpu.VMEM(shape, F32)

    dma = pltpu.SemaphoreType.DMA
    plane = nxc * ny - 1
    half = nz // 2
    ring = 2 * (6 + 6 * (half - 2) + 3)
    n_sends = ring + 5 * (nxc - 1) - (nxc - 1) + (ny - 1) * 7 + 3 * (nz - 1) + 2 * plane
    scratch = [
        vb(ny, 6, nz // ny, 16, q), vb(rows, q), vb(nxc, rows, q), vb(ny, rows, q),
        vb(ny, q, LANES), vb(ny, q, LANES), vb(ny, LANES, q), vf(nz * nxc, LANES), vf(nz, nxc, LANES),
        vb(width, width), vb(HEAD * HEAD, LANES), vb(rows, heads, HEAD * HEAD), vf(5, rows * heads, LANES),
        vb(rows * heads, HEAD * HEAD),
        vb(ny, nxc, 3, rows, LANES), vb(ny, 3, rows, width), vb(rows, q), vb(nxc, rows, q),
        vb(nxc, nz // 8, rows, LANES), vb(ny, nz // 8, rows, width), vb(ny, rows, q), vb(ny, rows, q),
        vb(nz, rows, q), vb(ny * q, LANES), vb(ny * q, LANES), vb(LANES, ny * q), vb(ny, rows, q), vb(ny, rows, q),
        vb(count, nz * rows), vb(count, nz * rows), vb(nxc, slots, q), vb(nxc, slots, q),
        vb(ny, count, 2 * LANES), vb(ny, count, 2 * LANES), vb(count, LANES), vb(ny, count, LANES),
        vb(nxc, slots, q), vb(nxc, slots, q), vb(nz, rows, q), vb(nz, rows, q),
        dma((n_sends,)), dma((2, half, 6)), dma((nxc,)), dma((ny,)), dma((ny,)), dma((ny,)), dma((ny,)), dma((nz,)),
        dma((nxc * ny,)), dma((nxc,)), dma((nxc * ny,)), dma((nz,)), dma((ny,)), dma((nxc,)), dma((ny,)), dma((ny,)),
        dma((nxc,)), dma((nz,)), dma((7,)),
    ]
    return pl.pallas_call(
        functools.partial(layer, sizes),
        out_shape=jax.ShapeDtypeStruct((rows, q), BF16),
        in_specs=[vmem] * 7 + [hbm] + [vmem] * 6 + [hbm] * 6,
        out_specs=vmem,
        scratch_shapes=scratch,
        compiler_params=pltpu.CompilerParams(
            collective_id=0, has_side_effects=True, vmem_limit_bytes=48 * 1024 * 1024
        ),
        name="layer",
    )(
        tokens, *turned, state, *line, routing,
        expert_gate[0], expert_up[0], expert_down[0], shared_gate, shared_up, shared_down,
    )


def solution(mesh):
    shape = SHAPE if SHAPE else (16, 4, 2, mesh.shape["tp"])
    torus = Mesh(mesh.devices.reshape(shape), AXES)
    placed = (
        P(EP, "tp"), P(EP, "tp", None), P("tp"),
        P("tp", EP), P("tp", EP), P("tp", EP), P("tp", EP), P("tp", EP),
        P("tp"), P("tp"), P("tp"), P("tp", EP), P(), P(EP, None), P(EP, None),
        P(EP, None, "tp"), P(EP, None, "tp"), P(EP, "tp", None), P(None, "tp"), P(None, "tp"), P("tp", None),
    )
    return jax.shard_map(body, mesh=torus, in_specs=placed, out_specs=P(EP, "tp"), check_vma=False)


SHAPE = None
```

time: 402 us -> 135 us (0.34)
  blocking collectives: 179 us -> 0 us
  Pallas kernels: 0 us -> 124 us
  waiting for transfers between devices: 112 us -> 0 us
  starting transfers between devices: 55.1 us -> 0 us
  local copies, waits for them, and re-layouts: 41.4 us -> 10.2 us
  matrix products: 7.65 us -> 0 us
  other arithmetic: 4.57 us -> 0.01 us
    all_to_all x6 -> x0, blocking collectives: 179 us -> none  [the longest x4 89.2 us: sent_to_all(): return lax.all_to_all(copies, axis, split_axis=0, concat_axis=0, tiled=True)]
    pallas_call x0 -> x1, Pallas kernels: none -> 124 us  [body(): pl.pallas_call(functools.partial(layer, sizes), out_shape=jax.ShapeDtypeS...]
    all_to_all x8 -> x0, waiting for transfers between devices: 112 us -> none  [the longest x2 55.1 us: sent_to_all(): return lax.all_to_all(copies, axis, split_axis=0, concat_axis=0, tiled=True)]
    all_to_all x8 -> x0, starting transfers between devices: 55.1 us -> none  [the longest x2 21.6 us: sent_to_all(): return lax.all_to_all(copies, axis, split_axis=0, concat_axis=0, tiled=True)]
    reshape x14 -> x0, local copies, waits for them, and re-layouts: 16.6 us -> none  [the longest x6 6.08 us: cut_along(): return jnp.moveaxis(array.reshape(*before, devices, -1, *after), dim, 0)]
    dot_general x9 -> x0, matrix products: 7.65 us -> none  [the longest x1 2.92 us: mixer_rows(): readout = jnp.einsum('nhvk,nhk->nhv', updated, receptance)]
    all_to_all x6 -> x0, local copies, waits for them, and re-layouts: 6.61 us -> none  [the longest x4 6.14 us: project_split(): lax.all_to_all(gathered, EP, split_axis=0, concat_axis=2, tiled=True)]
    unnamed x48 -> x43, local copies, waits for them, and re-layouts: 11.9 us -> 10.2 us
  transfers between devices with their start and end apart: 8 -> 0, of which waited for: 8 -> 0; matrix products, arithmetic and copies ran while one was open for 2% -> 0% of each run, Pallas kernels for 0% -> 0%
where the time goes in v1:
time: 135 us; the launch traced here: 134 us
  Pallas kernels  124 us (92%)
  local copies, waits for them, and re-layouts  10.2 us (8%)
    pallas_call x1, Pallas kernels, body(): pl.pallas_call(functools.partial(layer, sizes), out_shape=jax.ShapeDtypeS...  124 us
    unnamed x43, local copies, waits for them, and re-layouts  10.2 us

profile of v1, /device:TPU:1, one launch (start us, length us, event | category | flops | bytes accessed | tf_op | source)
XLA Modules:
  0.0 134.3 jit_solution(18367458281083707843)
XLA Ops:
  0.0 0.0 copy-start.19
  0.0 0.7 copy-done.19
  0.7 0.0 copy-start.20
  0.7 0.7 copy-done.20
  1.4 0.0 copy-start.14
  1.4 0.0 copy-start.15
  1.4 0.0 copy-start.16
  1.4 0.0 copy-start.17
  1.4 0.0 copy-start.18
  1.4 0.0 copy-start.10
  1.4 0.0 copy-start.11
  1.4 0.0 copy-start.12
  1.5 0.0 copy-start.13
  1.5 0.0 copy-start.7
  1.5 0.0 copy-start.8
  1.5 0.0 copy-start.9
  1.5 0.1 tile.10.routing
  1.6 0.5 copy-done.14
  2.1 0.0 copy-done.15
  2.1 0.0 copy-done.16
  2.1 0.0 copy-done.17
  2.1 0.0 copy-done.18
  2.1 0.1 copy-done.10
  2.2 0.0 copy-done.11
  2.2 0.0 copy-done.12
  2.2 0.0 copy-done.13
  2.2 0.0 copy-done.7
  2.2 0.0 copy-done.8
  2.3 0.0 copy-done.9
  2.3 0.0 copy-start
  2.3 1.2 copy-done
  3.5 0.0 copy-start.1
  3.5 1.0 copy-done.1
  4.5 0.0 copy-start.2
  4.5 1.0 copy-done.2
  5.6 0.0 copy-start.3
  5.6 1.0 copy-done.3
  6.6 0.0 copy-start.4
  6.6 1.0 copy-done.4
  7.7 0.0 copy-start.5
  7.7 1.0 copy-done.5
  8.7 0.0 copy-start.6
  8.7 1.0 copy-done.6
  9.8 123.9 %layer.1 = bf16[16,512]{1,0:T(8,128)(2,1)S(1)} custom-call(bf16[16,512]{1,0:T(8,128)(2,1)S(1)} %copy-done.7, bf16[16,512]{1,0:T(8,128)(2,1)S(1)} %bitcast.20, bf16[16,512]{1,0:T(8,128)(2,1)S(1)} %bitcast.21, bf16[16,512]{1,0:T(8,128)(2,1)S(1)} %bitcast.22, bf16[16,512]{1,0:T(8,128)(2,1)S(1)} %bitcast.23, bf16[16,512]{1,0:T(8,128)(2,1)S(1)} %bitcast.24, ...), custom_call_target="tpu_custom_call" | custom-call | tf_op jit(solution)/shard_map/layer/pallas_call | solution.py:424
  133.7 0.6 copy.23
  (3 shorter events, 0.0 us)
Async XLA Ops:
  0.0 0.7 copy-start.19
  0.7 0.7 copy-start.20
  1.4 0.7 copy-start.14
  1.4 0.7 copy-start.15
  1.4 0.7 copy-start.16
  1.4 0.7 copy-start.17
  1.4 0.7 copy-start.18
  1.4 0.8 copy-start.10
  1.4 0.8 copy-start.11
  1.4 0.8 copy-start.12
  1.5 0.8 copy-start.13
  1.5 0.8 copy-start.7
  1.5 0.8 copy-start.8
  1.5 0.8 copy-start.9
  2.3 1.2 copy-start
  3.5 1.0 copy-start.1
  4.5 1.0 copy-start.2
  5.6 1.0 copy-start.3
  6.6 1.0 copy-start.4
  7.7 1.0 copy-start.5
  8.7 1.0 copy-start.6

commit v2 on v1

v2 whole, which is shorter than its diff:
```python
import functools

import jax
import jax.numpy as jnp
from jax import lax
from jax.experimental import pallas as pl
from jax.experimental.pallas import tpu as pltpu
from jax.sharding import Mesh
from jax.sharding import PartitionSpec as P

HEAD = 64
LANES = 128
RMS_EPS = 1e-06
GN_EPS = 0.00064
KEY_EPS = 1e-06
ROUTED_SCALE = 2.5
AXES = ("ep_0", "ep_1", "ep_2", "tp")
EP = AXES[:3]
MESH_ID = pl.DeviceIdType.MESH
F32 = jnp.float32
BF16 = jnp.bfloat16
NT = (((1,), (1,)), ((), ()))
TN = (((0,), (0,)), ((), ()))


def iota(shape, dim):
    return lax.broadcasted_iota(jnp.int32, shape, dim)


def mm(a, b):
    return jnp.dot(a, b, preferred_element_type=F32)


def silu(v):
    return v * jax.nn.sigmoid(v)


def layer(
    sizes,
    tok_hbm, w0, w1, w2, w3, w4, w5, state, mix_hbm, dbase_hbm, rbase_hbm, hgain_hbm, mgain_hbm, routes_hbm, score_hbm,
    gate_hbm, up_hbm, down_hbm, sgate_hbm, sup_hbm, sdown_hbm,
    out,
    tok, mix_gain, decay_base, rate_base, head_gain, moe_gain, routes, score,
    wbuf, wo, xs, xg, tg, gt, ut, dt, vs, vg, perm, seg, st, nh, prod,
    ps, pr, ms, po, ar, resid, ns, zg, sgv, suv, sdv, sh, shr,
    dmat, cmat, xsel, er, gs, gr, hs, hr, ob, cb, rb, zr, zp, z8, za,
    s_send, s_ring, s_wx, s_wc, s_xg, s_tg, s_gt, s_ut, s_dt, s_vg, s_pr, s_ar, s_zg, s_shr, s_er, s_gr, s_hr, s_cb,
    s_zr, s_zp, s_z8, s_loc,
):
    nz, nx, nc, ny = sizes
    nxc = nx * nc
    rows, q = tok.shape
    zb = nz // ny
    heads = q // HEAD
    topk = routes.shape[0]
    weights = (w0, w1, w2, w3, w4, w5)
    half, quart = nz // 2, nz // 4
    order = [0, *[i for k in range(1, half) for i in (k, -k)], half]
    place = {r % nz: p for p, r in enumerate(order)}
    z, x, c, y = (lax.axis_index(a) for a in AXES)
    xc = x * nc + c
    sends = []

    def send(src, dst, recv_sem, where):
        copy = pltpu.make_async_remote_copy(
            src_ref=src, dst_ref=dst, send_sem=s_send.at[len(sends)], recv_sem=recv_sem,
            device_id=where, device_id_type=MESH_ID,
        )
        copy.start()
        sends.append(copy)

    def arrived(dst, recv_sem):
        pltpu.make_async_remote_copy(
            src_ref=dst, dst_ref=dst, send_sem=s_send.at[0], recv_sem=recv_sem,
            device_id=(z, x, c, y), device_id_type=MESH_ID,
        ).wait_recv()

    xc_off = [(dx, dc) for dx in range(nx) for dc in range(nc)]

    def xc_at(off):
        px, pc = lax.rem(x + off[0], nx), lax.rem(c + off[1], nc)
        return px, pc, px * nc + pc

    def y_at(dy):
        return lax.rem(y + dy, ny)

    def z_at(dz):
        return lax.rem(z + dz, nz)

    plane_off = [(o, dy) for o in xc_off for dy in range(ny)][1:]

    def at_lanes(i):
        return pl.ds(pl.multiple_of(i * LANES, LANES), LANES)

    local = []

    def load(src, dst):
        copy = pltpu.make_async_copy(src, dst, s_loc.at[len(local)])
        copy.start()
        local.append(copy)
        return copy

    def block(m, source):
        return wo.at[xc, source] if m == 5 else wbuf.at[source // zb, m, lax.rem(source, zb)]

    first = [load(tok_hbm, tok), load(mix_hbm, mix_gain), load(routes_hbm, routes), load(score_hbm, score)]
    own_w = [load(weights[m], block(m, z)) for m in range(6)]
    bases = [load(dbase_hbm, decay_base), load(rbase_hbm, rate_base), load(hgain_hbm, head_gain)]
    bases.append(load(mgain_hbm, moe_gain))
    load_state = load(state, st)
    own_rows = pl.ds(pl.multiple_of(y * q, q), q)
    load_gate = load(gate_hbm.at[own_rows, :], gt.at[y])
    load_up = load(up_hbm.at[own_rows, :], ut.at[y])
    load_down = load(down_hbm.at[:, own_rows], dt.at[y])
    load_sg = load(sgate_hbm, sgv)
    load_su = load(sup_hbm, suv)
    load_sd = load(sdown_hbm, sdv)

    width = nxc * LANES
    strip = nxc * 16
    for i in range(nxc):
        r = iota((LANES, width), 0)
        goal = (r // 16) * strip + i * 16 + lax.rem(r, 16)
        perm[i * LANES : (i + 1) * LANES, :] = (iota((LANES, width), 1) == goal).astype(BF16)
    for j in range(HEAD // 2):
        r = iota((LANES, LANES), 0)
        goal = 2 * j + r // HEAD
        seg[j * LANES : (j + 1) * LANES, :] = (lax.rem(iota((LANES, LANES), 1), HEAD) == goal).astype(BF16)

    for copy in first:
        copy.wait()
    rows_in = (tok[...].astype(F32) * mix_gain[...]).astype(BF16)
    xs[...] = rows_in
    xg[xc] = rows_in
    tg[y] = tok[...]

    spreader = (lax.rem(iota((rows, LANES), 1), rows) == iota((rows, LANES), 0)).astype(F32)
    exact = functools.partial(jnp.dot, preferred_element_type=F32, precision=lax.Precision.HIGHEST)
    share = score[...] / jnp.sum(score[...], axis=0, keepdims=True) * ROUTED_SCALE
    route_lanes = exact(routes[...].astype(F32), spreader)
    share_lanes = exact(share, spreader)
    experts = vs.shape[0]
    expert_id = iota((experts, LANES), 0).astype(F32)
    value = jnp.zeros((experts, LANES), F32)
    for k in range(topk):
        value += jnp.where(jnp.abs(expert_id - route_lanes[k : k + 1, :]) < 0.5, share_lanes[k : k + 1, :], 0.0)
    same_block = (iota((LANES, LANES), 0) // rows == iota((LANES, LANES), 1) // rows) & (
        iota((LANES, LANES), 0) < iota((LANES, LANES), 1)
    )
    before = mm((value > 0.0).astype(BF16), same_block.astype(BF16))
    vs[...] = jnp.where(before > 0.5, -value, value)
    for copy in own_w:
        copy.wait()

    barrier = pltpu.get_barrier_semaphore()
    for off, dy in plane_off:
        px, pc, _ = xc_at(off)
        pl.semaphore_signal(barrier, inc=1, device_id=(z, px, pc, y_at(dy)), device_id_type=MESH_ID)
    for dz in range(1, nz):
        pl.semaphore_signal(barrier, inc=1, device_id=(z_at(dz), x, c, y), device_id_type=MESH_ID)
    pl.semaphore_wait(barrier, len(plane_off) + nz - 1)

    to_next, to_prev = (z_at(1), x, c, y), (z_at(nz - 1), x, c, y)
    ring = (5, 0, 1, 2, 3, 4)
    split = ring[:3]
    for m in ring:
        spot = block(m, z)
        send(spot, spot, s_ring.at[0, 0, m], to_next)
        send(spot, spot, s_ring.at[1, 0, m], to_prev)

    def pass_along_x(source):
        for dx in range(1, nx):
            px = lax.rem(x + dx, nx)
            send(wo.at[xc, source], wo.at[xc, source], s_wx.at[x, source], (z, px, c, y))

    pass_along_x(z)
    for off in xc_off[1:]:
        px, pc, _ = xc_at(off)
        send(xs, xg.at[xc], s_xg.at[xc], (z, px, pc, y))
    for dy in range(1, ny):
        send(tok, tg.at[y], s_tg.at[y], (z, x, c, y_at(dy)))
    for dy in range(1, ny):
        theirs = pl.ds(pl.multiple_of(y_at(dy) * q, q), q)
        send(gate_hbm.at[theirs, :], gt.at[y], s_gt.at[y], (z, x, c, y_at(dy)))
        send(up_hbm.at[theirs, :], ut.at[y], s_ut.at[y], (z, x, c, y_at(dy)))
    for dy in range(1, ny):
        theirs = pl.ds(pl.multiple_of(y_at(dy) * q, q), q)
        send(down_hbm.at[:, theirs], dt.at[y], s_dt.at[y], (z, x, c, y_at(dy)))

    for step in range(1, half + 1):
        up_src, down_src = z_at(nz - step), z_at(step)
        for m in ring:
            if step < half or m in split:
                spot = block(m, up_src)
                arrived(spot, s_ring.at[0, step - 1, m])
                if step + 1 < half or (step + 1 == half and m in split):
                    send(spot, spot, s_ring.at[0, step, m], to_next)
                if m == 5:
                    pass_along_x(up_src)
            if step < half or m not in split:
                spot = block(m, down_src)
                arrived(spot, s_ring.at[1, step - 1, m])
                if step + 1 < half or (step + 1 == half and m not in split):
                    send(spot, spot, s_ring.at[1, step, m], to_prev)
                if m == 5:
                    pass_along_x(down_src)

    for off in xc_off[1:]:
        _, _, pxc = xc_at(off)
        arrived(xg.at[pxc], s_xg.at[pxc])
    left = xg[...].reshape(nxc * rows, q)
    for yt in range(ny):
        for pair in range(3):
            first_m = min(2 * pair, 3)
            w = wbuf[yt, first_m : first_m + 2].reshape(LANES, q)
            part = lax.dot_general(left, w, NT, preferred_element_type=F32)
            ps[yt, :, pair] = part.astype(BF16).reshape(nxc, rows, LANES)
    for off, dy in plane_off:
        px, pc, pxc = xc_at(off)
        py = y_at(dy)
        send(ps.at[py, pxc], pr.at[y, :, :, at_lanes(xc)], s_pr.at[xc * ny + y], (z, px, pc, py))
    def rows_of(zt):
        return vs.at[pl.ds(pl.multiple_of(zt * nxc, nxc), nxc), :]

    for r in range(1, nz):
        send(rows_of(z_at(r)), vg.at[place[-r % nz]], s_vg.at[place[-r % nz]], (z_at(r), x, c, y))
    vg[0] = vs[pl.ds(pl.multiple_of(z * nxc, nxc), nxc), :]
    pr[y, :, :, at_lanes(xc)] = ps[y, xc]

    for dy in range(1, ny):
        arrived(tg.at[y_at(dy)], s_tg.at[y_at(dy)])
    tok_all = tg[...].astype(F32)
    square = jnp.sum(jnp.sum(tok_all * tok_all, axis=0), axis=1, keepdims=True)
    factor = lax.rsqrt(square / (ny * q) + RMS_EPS)

    for off, dy in plane_off:
        _, _, pxc = xc_at(off)
        arrived(pr.at[y_at(dy), :, :, at_lanes(pxc)], s_pr.at[pxc * ny + y_at(dy)])
    for dx in range(1, nx):
        px = lax.rem(x + dx, nx)
        for source in range(nz):
            arrived(wo.at[px * nc + c, source], s_wx.at[px, source])
    for px in range(nx):
        for dc in range(1, nc):
            send(wo.at[px * nc + c], wo.at[px * nc + c], s_wc.at[px], (z, x, lax.rem(c + dc, nc), y))
    for copy in bases:
        copy.wait()
    spread = mm(pr[...].reshape(ny * 3 * rows, width), perm[...]).reshape(ny, 3, rows, width)
    summed = jnp.sum(spread, axis=0)
    low = iota((rows, LANES), 1) < HEAD
    for m in range(5):
        group, side = (2, 1) if m == 4 else (m // 2, m % 2)
        flat = summed[group, :, side * q : (side + 1) * q] * factor
        if m == 3:
            flat = flat + decay_base[...]
        if m == 4:
            flat = flat + rate_base[...]
        for t in range(q // LANES):
            here = flat[:, t * LANES : (t + 1) * LANES]
            swapped = pltpu.roll(here, HEAD, 1)
            nh[m, pl.ds(2 * t, rows, stride=heads), :] = jnp.where(low, here, swapped)
            nh[m, pl.ds(2 * t + 1, rows, stride=heads), :] = jnp.where(low, swapped, here)

    def head_sum(v):
        return 0.5 * jnp.sum(v, axis=1, keepdims=True)

    receptance, key, val = nh[0], nh[1], nh[2]
    decay = jnp.exp(-jnp.exp(-jax.nn.softplus(-nh[3]) - 0.5))
    in_rate = jax.nn.sigmoid(nh[4])
    unit = key * lax.rsqrt(head_sum(key * key) + KEY_EPS)
    rated = in_rate * receptance
    mix_w = decay * receptance - head_sum(unit * rated) * unit
    fed = head_sum(key * rated)
    load_state.wait()
    for j in range(HEAD // 2):
        block = st[:, :, j * LANES : (j + 1) * LANES].astype(F32).reshape(rows * heads, LANES)
        prod[:, j * LANES : (j + 1) * LANES] = (block * mix_w).astype(BF16)
    readout = mm(prod[...], seg[...]) + fed * val
    centre = jnp.sum(readout, axis=1, keepdims=True) / LANES
    moved = readout - centre
    var = jnp.sum(moved * moved, axis=1, keepdims=True) / LANES
    nh[0] = moved * lax.rsqrt(var + GN_EPS)
    for t in range(q // LANES):
        even = nh[0, pl.ds(2 * t, rows, stride=heads), :]
        odd = nh[0, pl.ds(2 * t + 1, rows, stride=heads), :]
        cols = slice(t * LANES, (t + 1) * LANES)
        ms[:, cols] = (jnp.where(low, even, odd) * head_gain[:, cols]).astype(BF16)

    for px in range(nx):
        for dc in range(1, nc):
            arrived(wo.at[px * nc + lax.rem(c + dc, nc)], s_wc.at[px])
    mixed = ms[...]
    for i in range(nxc):
        for zh in range(nz // 8):
            w = wo[i, 8 * zh : 8 * (zh + 1)].reshape(LANES, q)
            part = lax.dot_general(mixed, w, NT, preferred_element_type=F32)
            po[zh, :, i * LANES : (i + 1) * LANES] = part.astype(BF16)
    for dy in range(1, ny):
        send(po, ar.at[y], s_ar.at[y], (z, x, c, y_at(dy)))
    ar[y] = po[...]
    for dy in range(1, ny):
        arrived(ar.at[y_at(dy)], s_ar.at[y_at(dy)])
    spread = mm(ar[...].reshape(ny * (nz // 8) * rows, width), perm[...]).reshape(ny, nz // 8, rows, width)
    summed = jnp.sum(spread, axis=0)
    per = width // q
    square = jnp.zeros((rows, 1), F32)
    for i in range(ny):
        attended = summed[i // per, :, (i % per) * q : (i % per + 1) * q]
        resid[i] = (tg[i].astype(F32) + attended).astype(BF16)
        r32 = resid[i].astype(F32)
        square += jnp.sum(r32 * r32, axis=1, keepdims=True)
    factor = lax.rsqrt(square / (ny * q) + RMS_EPS)
    for i in range(ny):
        ns[i] = (resid[i].astype(F32) * factor * moe_gain[:, i * q : (i + 1) * q]).astype(BF16)

    for k in range(quart, 0, -1):
        for r in (k, -k):
            spot = place[-r % nz]
            send(ns.at[y], zg.at[spot], s_zg.at[spot], (z_at(r % nz), x, c, y))
    zg[0] = ns[y]

    load_sg.wait()
    load_su.wait()
    load_sd.wait()
    hid_g = jnp.zeros((rows, LANES), F32)
    hid_u = jnp.zeros((rows, LANES), F32)
    for i in range(ny):
        hid_g += mm(ns[i], sgv[i * q : (i + 1) * q, :])
        hid_u += mm(ns[i], suv[i * q : (i + 1) * q, :])
    hid = (silu(hid_g) * hid_u).astype(BF16)
    for i in range(ny):
        sh[i] = mm(hid, sdv[:, i * q : (i + 1) * q]).astype(BF16)
    for dy in range(1, ny):
        send(sh.at[y_at(dy)], shr.at[y], s_shr.at[y], (z, x, c, y_at(dy)))
    shr[y] = sh[y]

    for r in range(1, nz):
        arrived(vg.at[place[r]], s_vg.at[place[r]])
    lane_block = iota((nxc, LANES), 1) // rows
    shape = (2 * half, half * rows)
    mine = iota(shape, 0) // 2 == iota(shape, 1) // rows
    sign = jnp.where(lax.rem(iota(shape, 0), 2) == 0, 1.0, -1.0)
    for ch in range(2):
        table = jnp.zeros((nxc, LANES), F32)
        for p in range(half):
            table += jnp.where(lane_block == p, vg[ch * half + p], 0.0)
        for i in range(nxc):
            weight = jnp.where(mine, table[i : i + 1, 0 : half * rows] * sign, 0.0)
            spot = slice(i * 2 * half, (i + 1) * 2 * half)
            dmat[ch, spot, :] = (weight > 0.0).astype(BF16)
            cmat[ch, spot, :] = jnp.maximum(weight, 0.0).astype(BF16)

    def wait_zg(p):
        arrived(zg.at[p], s_zg.at[p])

    back, ahead = place[-quart % nz], place[quart]
    wait_zg(back)
    wait_zg(ahead)
    far = back + c * (ahead - back)
    spot = place[half]
    send(zg.at[far], zg.at[spot], s_zg.at[spot], (z_at(quart + c * (half if nc > 1 else 0)), x, c, y))
    for k in range(quart - 1, 0, -1):
        spot = place[-(quart + k) % nz]
        send(zg.at[back], zg.at[spot], s_zg.at[spot], (z_at(k), x, c, y))
        spot = place[quart + k]
        send(zg.at[ahead], zg.at[spot], s_zg.at[spot], (z_at(nz - k), x, c, y))

    def pick(ch):
        for p in range(ch * half, (ch + 1) * half):
            if p not in (0, back, ahead):
                wait_zg(p)
        chosen = mm(dmat[ch], zg[ch * half : (ch + 1) * half].reshape(half * rows, q)).astype(BF16)
        xsel[ch] = chosen.reshape(nxc, 2 * half, q)
        for off in xc_off[1:]:
            px, pc, pxc = xc_at(off)
            send(xsel.at[ch, pxc], er.at[ch, xc], s_er.at[ch, xc], (z, px, pc, y))
        er[ch, xc] = xsel[ch, xc]

    def gate_up(ch):
        for off in xc_off[1:]:
            _, _, pxc = xc_at(off)
            arrived(er.at[ch, pxc], s_er.at[ch, pxc])
        chosen = er[ch].reshape(nxc * 2 * half, q)
        for i in range(ny):
            gs[ch, i, :, 0:LANES] = mm(chosen, gt[i]).astype(BF16)
            gs[ch, i, :, LANES : 2 * LANES] = mm(chosen, ut[i]).astype(BF16)
        for dy in range(1, ny):
            send(gs.at[ch, y_at(dy)], gr.at[ch, y], s_gr.at[ch, y], (z, x, c, y_at(dy)))
        gr[ch, y] = gs[ch, y]

    def hidden(ch):
        for dy in range(1, ny):
            arrived(gr.at[ch, y_at(dy)], s_gr.at[ch, y_at(dy)])
        pre = jnp.sum(gr[ch].astype(F32), axis=0)
        hs[ch] = (silu(pre[:, 0:LANES]) * pre[:, LANES : 2 * LANES]).astype(BF16)
        for dy in range(1, ny):
            send(hs.at[ch], hr.at[ch, y], s_hr.at[ch, y], (z, x, c, y_at(dy)))
        hr[ch, y] = hs[ch]

    def down(ch):
        for dy in range(1, ny):
            arrived(hr.at[ch, y_at(dy)], s_hr.at[ch, y_at(dy)])
        total = mm(hr[ch, 0], dt[0])
        for i in range(1, ny):
            total += mm(hr[ch, i], dt[i])
        ob[ch] = total.astype(BF16).reshape(nxc, 2 * half, q)
        for off in xc_off[1:]:
            px, pc, pxc = xc_at(off)
            send(ob.at[ch, pxc], cb.at[ch, xc], s_cb.at[ch, xc], (z, px, pc, y))
        cb[ch, xc] = ob[ch, xc]

    def combine(ch):
        for off in xc_off[1:]:
            _, _, pxc = xc_at(off)
            arrived(cb.at[ch, pxc], s_cb.at[ch, pxc])
        back_rows = cb[ch].reshape(nxc * 2 * half, q)
        routed = lax.dot_general(cmat[ch], back_rows, TN, preferred_element_type=F32)
        rb[ch * half : (ch + 1) * half] = routed.astype(BF16).reshape(half, rows, q)
        for p in range(half * (ch + 1) - 1, half * ch - 1, -1):
            r = order[p]
            if 0 < abs(r) < quart:
                spot = place[-r % nz]
                send(rb.at[p], zr.at[spot], s_zr.at[spot], (z_at(r % nz), x, c, y))
            elif quart < abs(r) < half:
                way, hop = (0, r - quart) if r > 0 else (1, r + quart)
                send(rb.at[p], zp.at[way, abs(hop) - 1], s_zp.at[way, abs(hop) - 1], (z_at(hop % nz), x, c, y))
            elif r == half:
                send(rb.at[p], z8, s_z8, (z_at(quart + c * (half if nc > 1 else 0)), x, c, y))

    pick(0)
    load_gate.wait()
    load_up.wait()
    load_down.wait()
    for dy in range(1, ny):
        arrived(gt.at[y_at(dy)], s_gt.at[y_at(dy)])
        arrived(ut.at[y_at(dy)], s_ut.at[y_at(dy)])
        arrived(dt.at[y_at(dy)], s_dt.at[y_at(dy)])
    gate_up(0)
    pick(1)
    hidden(0)
    gate_up(1)
    down(0)
    hidden(1)
    combine(0)
    down(1)
    combine(1)

    for way in range(2):
        for k in range(quart - 1):
            arrived(zp.at[way, k], s_zp.at[way, k])
    arrived(z8, s_z8)
    for way, r in ((0, quart), (1, -quart)):
        mine_too = (1 - c).astype(F32) if way == 0 else c.astype(F32)
        joined = rb[place[r % nz]].astype(F32) + z8[...].astype(F32) * mine_too
        for k in range(quart - 1):
            joined += zp[way, k].astype(F32)
        za[way] = joined.astype(BF16)
        spot = place[-r % nz]
        send(za.at[way], zr.at[spot], s_zr.at[spot], (z_at(r % nz), x, c, y))
    final = resid[y].astype(F32) + rb[0].astype(F32)
    for dy in range(1, ny):
        arrived(shr.at[y_at(dy)], s_shr.at[y_at(dy)])
    final += jnp.sum(shr[...].astype(F32), axis=0)
    for k in range(1, quart + 1):
        for r in (k, -k):
            spot = place[r % nz]
            arrived(zr.at[spot], s_zr.at[spot])
            final += zr[spot].astype(F32)
    out[...] = final.astype(BF16)
    for copy in sends:
        copy.wait_send()


def body(
    tokens, state, mix_gain, w_recept, w_key, w_value, w_decay, w_rate, decay_base, rate_base, head_gain, w_out,
    moe_gain, routes, route_weight, expert_gate, expert_up, expert_down, shared_gate, shared_up, shared_down,
):
    sizes = tuple(lax.axis_size(a) for a in AXES)
    nz, nx, nc, ny = sizes
    nxc = nx * nc
    rows, q = tokens.shape
    heads = q // HEAD
    topk = routes.shape[1]
    turned = [w.T for w in (w_recept, w_key, w_value, w_decay, w_rate, w_out)]
    line = [v[None, :] for v in (mix_gain, decay_base, rate_base, head_gain, moe_gain)]
    vmem = pl.BlockSpec(memory_space=pltpu.VMEM)
    hbm = pl.BlockSpec(memory_space=pl.ANY)
    half = nz // 2
    slots = 2 * half
    count = nxc * slots
    width = nxc * LANES

    def vb(*shape):
        return pltpu.VMEM(shape, BF16)

    def vf(*shape):
        return pltpu.VMEM(shape, F32)

    dma = pltpu.SemaphoreType.DMA
    scratch = [
        vb(rows, q), vf(1, q), vf(1, q), vf(1, q), vf(1, q), vf(1, ny * q),
        pltpu.VMEM((topk, rows), jnp.int32), vf(topk, rows),
        vb(ny, 5, nz // ny, 16, q), vb(nxc, nz, 16, q), vb(rows, q), vb(nxc, rows, q), vb(ny, rows, q),
        vb(ny, q, LANES), vb(ny, q, LANES), vb(ny, LANES, q), vf(nz * nxc, LANES), vf(nz, nxc, LANES),
        vb(width, width), vb(HEAD * HEAD, LANES), vb(rows, heads, HEAD * HEAD), vf(5, rows * heads, LANES),
        vb(rows * heads, HEAD * HEAD),
        vb(ny, nxc, 3, rows, LANES), vb(ny, 3, rows, width), vb(rows, q),
        vb(nz // 8, rows, width), vb(ny, nz // 8, rows, width), vb(ny, rows, q), vb(ny, rows, q),
        vb(nz, rows, q), vb(ny * q, LANES), vb(ny * q, LANES), vb(LANES, ny * q), vb(ny, rows, q), vb(ny, rows, q),
        vb(2, count, half * rows), vb(2, count, half * rows), vb(2, nxc, slots, q), vb(2, nxc, slots, q),
        vb(2, ny, count, 2 * LANES), vb(2, ny, count, 2 * LANES), vb(2, count, LANES), vb(2, ny, count, LANES),
        vb(2, nxc, slots, q), vb(2, nxc, slots, q), vb(nz, rows, q), vb(nz, rows, q),
        vb(2, nz // 4 - 1, rows, q), vb(rows, q), vb(2, rows, q),
        dma((300,)), dma((2, half, 6)), dma((nx, nz)), dma((nx,)), dma((nxc,)), dma((ny,)), dma((ny,)), dma((ny,)),
        dma((ny,)), dma((nz,)), dma((nxc * ny,)), dma((ny,)), dma((nz,)), dma((ny,)), dma((2, nxc)), dma((2, ny)),
        dma((2, ny)), dma((2, nxc)), dma((nz,)), dma((2, nz // 4 - 1)), dma, dma((21,)),
    ]
    return pl.pallas_call(
        functools.partial(layer, sizes),
        out_shape=jax.ShapeDtypeStruct((rows, q), BF16),
        in_specs=[hbm] * 21,
        out_specs=vmem,
        scratch_shapes=scratch,
        compiler_params=pltpu.CompilerParams(
            collective_id=0, has_side_effects=True
        ),
        name="layer",
    )(
        tokens, *turned, state, *line, routes.T, route_weight.T,
        expert_gate[0], expert_up[0], expert_down[0], shared_gate, shared_up, shared_down,
    )


def solution(mesh):
    shape = SHAPE if SHAPE else (16, 4, 2, mesh.shape["tp"])
    torus = Mesh(mesh.devices.reshape(shape), AXES)
    placed = (
        P(EP, "tp"), P(EP, "tp", None), P("tp"),
        P("tp", EP), P("tp", EP), P("tp", EP), P("tp", EP), P("tp", EP),
        P("tp"), P("tp"), P("tp"), P("tp", EP), P(), P(EP, None), P(EP, None),
        P(EP, None, "tp"), P(EP, None, "tp"), P(EP, "tp", None), P(None, "tp"), P(None, "tp"), P("tp", None),
    )
    return jax.shard_map(body, mesh=torus, in_specs=placed, out_specs=P(EP, "tp"), check_vma=False)


SHAPE = None
```

time: 135 us -> 111 us (0.82)
  Pallas kernels: 124 us -> 109 us
  local copies, waits for them, and re-layouts: 10.2 us -> 1.32 us
    pallas_call x1, Pallas kernels: 124 us -> 109 us  [body(): pl.pallas_call(functools.partial(layer, sizes), out_shape=jax.ShapeDtypeS...]
    unnamed x43 -> x1, local copies, waits for them, and re-layouts: 10.2 us -> 1.32 us
where the time goes in v2:
time: 111 us; the launch traced here: 110 us
  Pallas kernels  109 us (98%)
  local copies, waits for them, and re-layouts  1.32 us (1%)
    pallas_call x1, Pallas kernels, body(): pl.pallas_call(functools.partial(layer, sizes), out_shape=jax.ShapeDtypeS...  109 us

profile of v2, /device:TPU:1, one launch (start us, length us, event | category | flops | bytes accessed | tf_op | source)
XLA Modules:
  0.0 110.3 jit_solution(3395104931332621509)
XLA Ops:
  0.0 109.0 %layer.1 = bf16[16,512]{1,0:T(8,128)(2,1)} custom-call(bf16[16,512]{1,0:T(8,128)(2,1)} %tok_hbm.1, bf16[16,512]{1,0:T(8,128)(2,1)} %bitcast.19, bf16[16,512]{1,0:T(8,128)(2,1)} %bitcast.20, bf16[16,512]{1,0:T(8,128)(2,1)} %bitcast.21, bf16[16,512]{1,0:T(8,128)(2,1)} %bitcast.22, bf16[16,512]{1,0:T(8,128)(2,1)} %bitcast.23, bf16[16,512]{1,0:T(8,128)(2,1)} %bitcast.24, ...), custom_call_target="tpu_custom_call" | custom-call | tf_op jit(solution)/shard_map/layer/pallas_call | solution.py:518
  109.0 1.3 %copy.23 = bf16[16,512]{1,0:T(8,128)(2,1)} copy(bf16[16,512]{1,0:T(8,128)(2,1)} %layer.1) | data formatting | bytes 32768
